TPU v7x, 32 devices: a whole 2x2x4 slice. The times are simulated.
32 devices in a mesh: sp: 4 (over y, core), dp: 8 (over z, x).
Axes of the slice: x: 2, y: 2, z: 4, core: 2. Of those that a mesh axis runs over, the one named last changes fastest.
Arguments:
- queries: bfloat16 [8, 1024, 1024], P('dp', 'sp'), may hold values from -250 to 250
- keys: bfloat16 [8, 1024, 1024], P('dp', 'sp'), may hold values from -6 to 6
- values: bfloat16 [8, 1024, 1024], P('dp', 'sp'), may hold values from -6 to 6
- cum_gate: float32 [8, 16, 1024], P('dp', 'sp'), may hold values from -1024 to 0, as said below
- out_weight: bfloat16 [1024, 2112], P(None, 'dp'), may hold values from -1.5 to 1.5
Outputs:
- mixed: bfloat16 [8, 1024, 2112], P('dp', 'sp')
Inputs may be any that keep to these rules, and one draw needn't show every extreme that they name: `cum_gate`: within each head the entries do not rise along positions.
All inputs are finite; a program needn't handle non-finite values.
Results may differ from a plain program's by a relative error of at most 0.0053.
Values may be sent and summed in bfloat16 or wider, within the bound.
A program may use at most 64 MiB of HBM per device.

v0:
```python
import jax
import jax.numpy as jnp
from jax import lax
from jax.sharding import PartitionSpec as P


def attend(query_all, key_all, value_all, gate_all):
    length, width = query_all.shape
    heads = gate_all.shape[0]
    depth = width // heads
    block_rows = min(512, length)
    block_count = length // block_rows
    score_scale = depth ** (-0.5)
    query_blocks = query_all.reshape(block_count, block_rows, heads, depth)
    key_blocks = key_all.reshape(block_count, block_rows, heads, depth)
    value_blocks = value_all.reshape(block_count, block_rows, heads, depth)
    gate_blocks = gate_all.reshape(heads, block_count, block_rows).transpose(1, 0, 2)
    offsets = jnp.arange(block_rows, dtype=jnp.int32)

    def one_block(block_index):
        query_part = lax.dynamic_index_in_dim(query_blocks, block_index, 0, keepdims=False)
        gate_part = lax.dynamic_index_in_dim(gate_blocks, block_index, 0, keepdims=False)
        query_rows = block_index * block_rows + offsets

        def key_step(key_block, carry):
            running_max, running_sum, weighted = carry
            key_part = lax.dynamic_index_in_dim(key_blocks, key_block, 0, keepdims=False)
            value_part = lax.dynamic_index_in_dim(value_blocks, key_block, 0, keepdims=False)
            gate_keys = lax.dynamic_index_in_dim(gate_blocks, key_block, 0, keepdims=False)
            logits = (
                jnp.einsum("qhe,khe->hqk", query_part, key_part, preferred_element_type=jnp.float32)
                * score_scale
            )
            logits = logits + gate_part[:, :, None] - gate_keys[:, None, :]
            key_rows = key_block * block_rows + offsets
            allowed = key_rows[None, :] <= query_rows[:, None]
            logits = jnp.where(allowed[None], logits, -jnp.inf)
            new_max = jnp.maximum(running_max, jnp.max(logits, axis=-1))
            scores = jnp.exp(logits - new_max[..., None])
            factor = jnp.exp(running_max - new_max)
            running_sum = running_sum * factor + jnp.sum(scores, axis=-1)
            weighted = weighted * factor[..., None] + jnp.einsum(
                "hqk,khe->hqe",
                scores.astype(jnp.bfloat16),
                value_part,
                preferred_element_type=jnp.float32,
            )
            return (new_max, running_sum, weighted)

        start_state = (
            jnp.full((heads, block_rows), -jnp.inf, jnp.float32),
            jnp.zeros((heads, block_rows), jnp.float32),
            jnp.zeros((heads, block_rows, depth), jnp.float32),
        )
        final_max, final_sum, weighted = lax.fori_loop(0, block_index + 1, key_step, start_state)
        result = weighted / final_sum[..., None]
        return result.transpose(1, 0, 2).astype(jnp.bfloat16)

    outputs = lax.map(one_block, jnp.arange(block_count, dtype=jnp.int32))
    return outputs.reshape(length, width)


def body(queries, keys, values, cum_gate, out_weight):
    query_heads, key_heads, value_heads = (
        lax.all_to_all(queries, "sp", split_axis=2, concat_axis=1, tiled=True),
        lax.all_to_all(keys, "sp", split_axis=2, concat_axis=1, tiled=True),
        lax.all_to_all(values, "sp", split_axis=2, concat_axis=1, tiled=True),
    )
    local_out = attend(query_heads[0], key_heads[0], value_heads[0], cum_gate[0])
    attended = lax.all_to_all(local_out[None], "sp", split_axis=1, concat_axis=2, tiled=True)[0]
    group_rows = attended.shape[1] // lax.axis_size("sp")
    own_rows = lax.dynamic_slice_in_dim(
        out_weight, lax.axis_index("sp") * group_rows, group_rows, 0
    )
    full_rows = lax.all_gather(own_rows, "dp", axis=1, tiled=True)
    whole_weight = lax.all_gather(full_rows, "sp", axis=0, tiled=True)
    mixed = jnp.dot(attended, whole_weight, preferred_element_type=jnp.float32)
    return mixed.astype(jnp.bfloat16)[None]


def solution(mesh):
    in_specs = (
        P("dp", "sp", None),
        P("dp", "sp", None),
        P("dp", "sp", None),
        P("dp", "sp", None),
        P(None, "dp"),
    )
    out_specs = P("dp", "sp", None)
    return jax.shard_map(body, mesh=mesh, in_specs=in_specs, out_specs=out_specs, check_vma=False)
```

profile of v0, /device:TPU:0, one launch (start us, length us, event | category | flops | bytes accessed | tf_op | source)
XLA Modules:
  0.0 110.8 jit_solution(6020720090809697798)
XLA Ops:
  8.3 2.4 %copy.29 = bf16[1,256,1024]{1,0,2:T(2,128)(2,1)S(1)} copy(bf16[1,256,1024]{2,1,0:T(8,128)(2,1)} %param.9) | data formatting | bytes 1048576 | tf_op args[0]
  11.2 3.8 %reduce = bf16[1024,256]{1,0:T(8,128)(2,1)S(1)} reduce(bf16[1024,1,256]{2,1,0:T(2,128)(2,1)S(1)} %bitcast.91, bf16[]{:T(256)} %broadcast.54), dimensions={1}, to_apply=%bitcast.52.reduce_sub_computation | reduce | bytes 1048578
  15.9 4.3 %all-to-all-start = ((bf16[4,2,32768]{2,1,0:T(2,128)(2,1)}), bf16[4,2,32768]{2,1,0:T(2,128)(2,1)S(1)}, u32[]{:S(2)}, u32[]{:S(2)}) async-start(bf16[4,2,32768]{2,1,0:T(2,128)(2,1)} %reshape.40), calls=%async_computation | async-start | bytes 1048576 | tf_op jit(solution)/shard_map/all_to_all | solution.py:65
  21.0 3.8 %reduce.1 = bf16[1024,256]{1,0:T(8,128)(2,1)S(1)} reduce(bf16[1024,1,256]{2,1,0:T(2,128)(2,1)S(1)} %bitcast.93, bf16[]{:T(256)} %broadcast.54), dimensions={1}, to_apply=%bitcast.54.reduce_sub_computation | reduce | bytes 1048578
  25.8 3.2 %all-to-all-done = bf16[4,2,32768]{2,1,0:T(2,128)(2,1)S(1)} async-done(((bf16[4,2,32768]{2,1,0:T(2,128)(2,1)}), bf16[4,2,32768]{2,1,0:T(2,128)(2,1)S(1)}, u32[]{:S(2)}, u32[]{:S(2)}) %all-to-all-start) | async-done | bytes 524320 | tf_op jit(solution)/shard_map/all_to_all | solution.py:65
  29.0 3.5 %all-to-all-start.1 = ((bf16[4,2,32768]{2,1,0:T(2,128)(2,1)}), bf16[4,2,32768]{2,1,0:T(2,128)(2,1)S(1)}, u32[]{:S(2)}, u32[]{:S(2)}) async-start(bf16[4,2,32768]{2,1,0:T(2,128)(2,1)} %reshape.42), calls=%async_computation.1 | async-start | bytes 1048576 | tf_op jit(solution)/shard_map/all_to_all | solution.py:66
  32.5 2.4 %copy.33 = bf16[1,256,1024]{1,0,2:T(2,128)(2,1)S(1)} copy(bf16[1,256,1024]{2,1,0:T(8,128)(2,1)} %param.11) | data formatting | bytes 1048576 | tf_op args[2]
  34.9 3.8 %reduce.2 = bf16[1024,256]{1,0:T(8,128)(2,1)S(1)} reduce(bf16[1024,1,256]{2,1,0:T(2,128)(2,1)S(1)} %bitcast.94, bf16[]{:T(256)} %broadcast.54), dimensions={1}, to_apply=%bitcast.56.reduce_sub_computation | reduce | bytes 1048578
  39.6 1.7 %all-to-all-done.1 = bf16[4,2,32768]{2,1,0:T(2,128)(2,1)S(1)} async-done(((bf16[4,2,32768]{2,1,0:T(2,128)(2,1)}), bf16[4,2,32768]{2,1,0:T(2,128)(2,1)S(1)}, u32[]{:S(2)}, u32[]{:S(2)}) %all-to-all-start.1) | async-done | bytes 524320 | tf_op jit(solution)/shard_map/all_to_all | solution.py:66
  41.3 4.1 %all-to-all-start.2 = ((bf16[4,2,32768]{2,1,0:T(2,128)(2,1)}), bf16[4,2,32768]{2,1,0:T(2,128)(2,1)}, u32[]{:S(2)}, u32[]{:S(2)}) async-start(bf16[4,2,32768]{2,1,0:T(2,128)(2,1)} %reshape.44), calls=%async_computation.2 | async-start | bytes 1048576 | tf_op jit(solution)/shard_map/all_to_all | solution.py:67
  48.6 5.7 %all-to-all-done.2 = bf16[4,2,32768]{2,1,0:T(2,128)(2,1)} async-done(((bf16[4,2,32768]{2,1,0:T(2,128)(2,1)}), bf16[4,2,32768]{2,1,0:T(2,128)(2,1)}, u32[]{:S(2)}, u32[]{:S(2)}) %all-to-all-start.2) | async-done | bytes 524320 | tf_op jit(solution)/shard_map/all_to_all | solution.py:67
  54.3 2.2 %reshape.45 = bf16[1024,1,256]{2,1,0:T(2,128)(2,1)S(1)} reshape(bf16[4,2,32768]{2,1,0:T(2,128)(2,1)} %all-to-all-done.2) | data formatting | bytes 1048576
  58.3 21.7 %while.29 = (s32[]{:T(128)}, bf16[2,512,4,64]{1,3,2,0:T(8,128)(2,1)S(1)}, s32[2]{0:T(128)S(1)}, bf16[2,512,4,64]{1,3,2,0:T(8,128)(2,1)S(1)}, f32[2,4,512]{2,1,0:...) while((s32[]{:T(128)}, ...), condition=%wide.region_5.6_spmd.clone.clone, body=%wide.region_0.5_spmd.clone.clone.sunk | while | flops 287052800 | bytes 19649152 | solution.py:59
  62.2 4.6 %while.30 = (s32[]{:T(128)}, f32[4,512]{1,0:T(4,128)S(1)}, f32[4,512]{1,0:T(4,128)S(1)}, f32[4,512,64]{1,2,0:T(8,128)S(1)}, s32[]{:T(128)}, /*index=5*/s32[512]{...) while((s32[]{:T(128)}, f32[4,512]{1,0:T(4,128)S(1)}, ...), condition=%wide.region_4.4_spmd, body=%wide.region_1.3_spmd.sunk | while | flops 286790144 | bytes 17768688 | solution.py:55
  63.8 1.4 %fusion.34 = f32[4,512]{1,0:T(4,128)S(1)} fusion(f32[4,512,512]{2,1,0:T(8,128)S(1)} %get-tuple-element.369, f32[4,512]{1,0:T(4,128)S(1)} %max.4, f32[4,512]{1,0:T(4,128)S(1)} %dynamic-slice_bitcast_fusion.8, f32[4,512]{1,0:T(4,128)S(1)} %get-tuple-element.413, pred[512,512]{0,1:T(8,128)(4,1)S(1)} %broadcast_compare_fusion.2), kind=kLoop, calls=%fused_computation.4.clone.1 | loop fusion | flops 6289408 | bytes 4489216 | tf_op jit(solution)/shard_map/while/body/eval_jaxpr/while/body/reduce_sum | solution.py:41
  65.2 1.6 %fusion.35 = f32[4,512,64]{1,2,0:T(8,128)S(1)} fusion(f32[4,512,512]{2,1,0:T(8,128)S(1)} %get-tuple-element.369, f32[4,512]{1,0:T(4,128)S(1)} %max.4, f32[4,512]{1,0:T(4,128)S(1)} %dynamic-slice_bitcast_fusion.8, f32[4,512]{1,0:T(4,128)S(1)} %get-tuple-element.413, pred[512,512]{0,1:T(8,128)(4,1)S(1)} %broadcast_compare_fusion.2, ...), kind=kOutput, calls=%fused_computation.8.clone.1 | convolution fusion | flops 140771328 | bytes 5799940 | tf_op jit(solution)/shard_map/while/body/eval_jaxpr/while/body/hqk,khe->hqe/dot_general | solution.py:42
  70.8 9.1 %while.30 = (s32[]{:T(128)}, f32[4,512]{1,0:T(4,128)S(1)}, f32[4,512]{1,0:T(4,128)S(1)}, f32[4,512,64]{1,2,0:T(8,128)S(1)}, s32[]{:T(128)}, /*index=5*/s32[512]{...) while((s32[]{:T(128)}, f32[4,512]{1,0:T(4,128)S(1)}, ...), condition=%wide.region_4.4_spmd, body=%wide.region_1.3_spmd.sunk | while | flops 286790144 | bytes 17768688 | solution.py:55
  72.4 1.4 %fusion.34 = f32[4,512]{1,0:T(4,128)S(1)} fusion(f32[4,512,512]{2,1,0:T(8,128)S(1)} %get-tuple-element.369, f32[4,512]{1,0:T(4,128)S(1)} %max.4, f32[4,512]{1,0:T(4,128)S(1)} %dynamic-slice_bitcast_fusion.8, f32[4,512]{1,0:T(4,128)S(1)} %get-tuple-element.413, pred[512,512]{0,1:T(8,128)(4,1)S(1)} %broadcast_compare_fusion.2), kind=kLoop, calls=%fused_computation.4.clone.1 | loop fusion | flops 6289408 | bytes 4489216 | tf_op jit(solution)/shard_map/while/body/eval_jaxpr/while/body/reduce_sum | solution.py:41
  73.8 1.6 %fusion.35 = f32[4,512,64]{1,2,0:T(8,128)S(1)} fusion(f32[4,512,512]{2,1,0:T(8,128)S(1)} %get-tuple-element.369, f32[4,512]{1,0:T(4,128)S(1)} %max.4, f32[4,512]{1,0:T(4,128)S(1)} %dynamic-slice_bitcast_fusion.8, f32[4,512]{1,0:T(4,128)S(1)} %get-tuple-element.413, pred[512,512]{0,1:T(8,128)(4,1)S(1)} %broadcast_compare_fusion.2, ...), kind=kOutput, calls=%fused_computation.8.clone.1 | convolution fusion | flops 140771328 | bytes 5799940 | tf_op jit(solution)/shard_map/while/body/eval_jaxpr/while/body/hqk,khe->hqe/dot_general | solution.py:42
  77.0 1.4 %fusion.34 = f32[4,512]{1,0:T(4,128)S(1)} fusion(f32[4,512,512]{2,1,0:T(8,128)S(1)} %get-tuple-element.369, f32[4,512]{1,0:T(4,128)S(1)} %max.4, f32[4,512]{1,0:T(4,128)S(1)} %dynamic-slice_bitcast_fusion.8, f32[4,512]{1,0:T(4,128)S(1)} %get-tuple-element.413, pred[512,512]{0,1:T(8,128)(4,1)S(1)} %broadcast_compare_fusion.2), kind=kLoop, calls=%fused_computation.4.clone.1 | loop fusion | flops 6289408 | bytes 4489216 | tf_op jit(solution)/shard_map/while/body/eval_jaxpr/while/body/reduce_sum | solution.py:41
  78.4 1.6 %fusion.35 = f32[4,512,64]{1,2,0:T(8,128)S(1)} fusion(f32[4,512,512]{2,1,0:T(8,128)S(1)} %get-tuple-element.369, f32[4,512]{1,0:T(4,128)S(1)} %max.4, f32[4,512]{1,0:T(4,128)S(1)} %dynamic-slice_bitcast_fusion.8, f32[4,512]{1,0:T(4,128)S(1)} %get-tuple-element.413, pred[512,512]{0,1:T(8,128)(4,1)S(1)} %broadcast_compare_fusion.2, ...), kind=kOutput, calls=%fused_computation.8.clone.1 | convolution fusion | flops 140771328 | bytes 5799940 | tf_op jit(solution)/shard_map/while/body/eval_jaxpr/while/body/hqk,khe->hqe/dot_general | solution.py:42
  81.4 3.8 %reduce.3 = bf16[1024,256]{1,0:T(8,128)(2,1)S(1)} reduce(bf16[1024,1,256]{2,1,0:T(2,128)(2,1)S(1)} %bitcast.92, bf16[]{:T(256)} %broadcast.54), dimensions={1}, to_apply=%bitcast.58.reduce_sub_computation | reduce | bytes 1048578
  85.4 13.2 %all_to_all.60 = bf16[4,2,32768]{2,1,0:T(2,128)(2,1)S(1)} all-to-all(bf16[4,2,32768]{2,1,0:T(2,128)(2,1)S(1)} %reshape.46), channel_id=1, replica_groups=mesh['sp'=4,'dp'=8] {'sp'}, dimensions={0} | all-to-all | bytes 1048576 | tf_op jit(solution)/shard_map/all_to_all | solution.py:70
  99.4 4.5 %fusion.20 = bf16[1,256,2112]{1,2,0:T(8,128)(2,1)} fusion(bf16[1024,2112]{0,1:T(8,128)(2,1)} %all-gather.5.cloned.1.call-done, bf16[256,1024]{0,1:T(8,128)(2,1)S(1)} %bitcast.100), kind=kOutput, calls=%fused_computation.29 | convolution fusion | flops 1107836928 | bytes 5931008 | tf_op jit(solution)/shard_map/dot_general | solution.py:77
  (87 shorter events, 19.1 us)
Async XLA Ops:
  6.5 1.0 copy-start
  6.5 13.7 %copy-start.2 = (bf16[1,256,1024]{2,1,0:T(8,128)(2,1)S(1)}, bf16[1,256,1024]{2,1,0:T(8,128)(2,1)}, u32[]{:S(2)}) copy-start(bf16[1,256,1024]{2,1,0:T(8,128)(2,1)} %param.10) | copy-start | bytes 1572868
  6.5 51.7 %all-gather.3.cloned.1.call-start = ((), (), s32[]{:S(2)}) async-start(), calls=%async_computation.4 | async-start | bytes 1216512 | tf_op jit(solution)/shard_map/all_gather | solution.py:75
  15.9 13.1 %all-to-all-start = ((bf16[4,2,32768]{2,1,0:T(2,128)(2,1)}), bf16[4,2,32768]{2,1,0:T(2,128)(2,1)S(1)}, u32[]{:S(2)}, u32[]{:S(2)}) async-start(bf16[4,2,32768]{2,1,0:T(2,128)(2,1)} %reshape.40), calls=%async_computation | async-start | bytes 1048576 | tf_op jit(solution)/shard_map/all_to_all | solution.py:65
  29.0 12.3 %all-to-all-start.1 = ((bf16[4,2,32768]{2,1,0:T(2,128)(2,1)}), bf16[4,2,32768]{2,1,0:T(2,128)(2,1)S(1)}, u32[]{:S(2)}, u32[]{:S(2)}) async-start(bf16[4,2,32768]{2,1,0:T(2,128)(2,1)} %reshape.42), calls=%async_computation.1 | async-start | bytes 1048576 | tf_op jit(solution)/shard_map/all_to_all | solution.py:66
  41.3 13.0 %all-to-all-start.2 = ((bf16[4,2,32768]{2,1,0:T(2,128)(2,1)}), bf16[4,2,32768]{2,1,0:T(2,128)(2,1)}, u32[]{:S(2)}, u32[]{:S(2)}) async-start(bf16[4,2,32768]{2,1,0:T(2,128)(2,1)} %reshape.44), calls=%async_computation.2 | async-start | bytes 1048576 | tf_op jit(solution)/shard_map/all_to_all | solution.py:67
  45.4 54.0 %all-gather.5.cloned.1.call-start = ((), (), s32[]{:S(2)}) async-start(), calls=%async_computation.5 | async-start | bytes 5406720 | tf_op jit(solution)/shard_map/all_gather | solution.py:76
  48.5 9.8 %copy-start.1 = (f32[1,4,1024]{2,1,0:T(4,128)S(1)}, f32[1,4,1024]{2,1,0:T(4,128)}, u32[]{:S(2)}) copy-start(f32[1,4,1024]{2,1,0:T(4,128)} %param.12) | copy-start | bytes 49156
  48.5 9.8 %copy-start.3 = (bf16[2,512,4,64]{1,3,2,0:T(8,128)(2,1)S(1)}, bf16[2,512,4,64]{1,3,2,0:T(8,128)(2,1)}, u32[]{:S(2)}) copy-start(bf16[2,512,4,64]{1,3,2,0:T(8,128)(2,1)} %custom-call) | copy-start | bytes 1572868
  62.5 2.7 %copy-start.4 = (bf16[2,512,4,64]{1,3,2,0:T(8,128)(2,1)S(1)}, bf16[2,512,4,64]{1,3,2,0:T(8,128)(2,1)}, u32[]{:S(2)}) copy-start(bf16[2,512,4,64]{1,3,2,0:T(8,128)(2,1)} %get-tuple-element.415) | copy-start | bytes 1572868 | tf_op jit(solution)/shard_map/while/body/eval_jaxpr/while
  71.1 2.7 %copy-start.4 = (bf16[2,512,4,64]{1,3,2,0:T(8,128)(2,1)S(1)}, bf16[2,512,4,64]{1,3,2,0:T(8,128)(2,1)}, u32[]{:S(2)}) copy-start(bf16[2,512,4,64]{1,3,2,0:T(8,128)(2,1)} %get-tuple-element.415) | copy-start | bytes 1572868 | tf_op jit(solution)/shard_map/while/body/eval_jaxpr/while
  75.7 2.7 %copy-start.4 = (bf16[2,512,4,64]{1,3,2,0:T(8,128)(2,1)S(1)}, bf16[2,512,4,64]{1,3,2,0:T(8,128)(2,1)}, u32[]{:S(2)}) copy-start(bf16[2,512,4,64]{1,3,2,0:T(8,128)(2,1)} %get-tuple-element.415) | copy-start | bytes 1572868 | tf_op jit(solution)/shard_map/while/body/eval_jaxpr/while
Sparse Core Ops, SparseCore 0:
  9.5 43.1 all-gather.2
  58.4 38.7 all-gather.4
where the time goes:
time: 111 us
  local copies, waits for them, and re-layouts  21.2 us (19%)
  other arithmetic  20.1 us (18%)
  between operations  13.7 us (12%)
  blocking collectives  13.2 us (12%)
  matrix products  13 us (12%)
  starting transfers between devices  12.1 us (11%)
  waiting for transfers between devices  10.6 us (10%)
  loops' own time  6.82 us (6%)
    unnamed x27, local copies, waits for them, and re-layouts  15.3 us
    unnamed x4, other arithmetic  15.2 us
    all_to_all x1, blocking collectives, body(): lax.all_to_all(local_out[None], 'sp', split_axis=1, concat_axis=2, tiled=...  13.2 us
    another operation x1, loops' own time, attend(): outputs = lax.map(one_block, jnp.arange(block_count, dtype=jnp.int32))  6.51 us
    all_to_all x1, waiting for transfers between devices, body(): lax.all_to_all(values, 'sp', split_axis=2, concat_axis=1, tiled=True)  5.69 us
    dot_general x3, matrix products, key_step(): jnp.einsum('hqk,khe->hqe', scores.astype(jnp.bfloat16), value_part, prefe...  4.72 us
    dot_general x1, matrix products, body(): mixed = jnp.dot(attended, whole_weight, preferred_element_type=jnp.float32)  4.5 us
    all_to_all x1, starting transfers between devices, body(): lax.all_to_all(queries, 'sp', split_axis=2, concat_axis=1, tiled=True)  4.26 us
  transfers between devices with their start and end apart: 5, of which 3 were waited for; matrix products, arithmetic and copies ran while one was open for 43% of the time, Pallas kernels for 0%

commit v1 on v0

--- a/solution.py
+++ b/solution.py
@@ -1,7 +1,298 @@
+import functools
+import math
+
 import jax
 import jax.numpy as jnp
 from jax import lax
+from jax.experimental import pallas as pl
+from jax.experimental.pallas import tpu as pltpu
 from jax.sharding import PartitionSpec as P
+
+LANES = 128
+SUBLANES = 16
+MESH = pl.DeviceIdType.MESH
+
+
+def ring_index(position, n):
+    upper = position // (n // 2)
+    return (1 - upper) * (2 * position) + upper * (2 * (n - 1 - position) + 1)
+
+
+def fused_kernel(
+    sp, dp, depth, q, k, v, gate, w, tail, out,
+    qg, kg, vg, og, attended, wg,
+    qkv_send, qkv_recv, qkv_local, out_send, out_recv, out_local,
+    ring_send, ring_recv, pair_send, pair_recv, own_sem,
+):
+    tokens, width = q.shape
+    group = width // sp
+    pairs = group // LANES
+    per_pair = LANES // depth
+    half_rows = width // 2
+    main = wg.shape[3]
+    rows = wg.shape[2]
+    tail_rows = rows - half_rows
+    columns = w.shape[1]
+    tail_columns = columns - main
+    steps = dp // 2
+    cut = -(-(rows // 2) // SUBLANES) * SUBLANES
+    me = lax.axis_index("sp")
+    mine = lax.axis_index("dp")
+    core = lax.rem(me, 2)
+    partner = me + 1 - 2 * core
+    odd = lax.rem(mine, 2)
+    position = (1 - odd) * (mine // 2) + odd * (dp - 1 - mine // 2)
+    right = ring_index(lax.rem(position + 1, dp), dp)
+    left = ring_index(lax.rem(position + dp - 1, dp), dp)
+
+    barrier = pltpu.get_barrier_semaphore()
+    for d in range(1, sp):
+        pl.semaphore_signal(
+            barrier, inc=1, device_id=(lax.rem(me + d, sp), mine), device_id_type=MESH
+        )
+    for side in (left, right):
+        pl.semaphore_signal(barrier, inc=1, device_id=(me, side), device_id_type=MESH)
+
+    own_copies = []
+    for half in range(2):
+        own_copies.append(pltpu.make_async_copy(
+            w.at[pl.ds(half * half_rows, half_rows), pl.ds(0, main)],
+            wg.at[mine, half, pl.ds(0, half_rows)], own_sem.at[half]))
+        own_copies.append(pltpu.make_async_copy(
+            tail.at[half], wg.at[mine, half, pl.ds(half_rows, tail_rows)],
+            own_sem.at[2 + half]))
+    local_copies = {}
+    arrays = ((q, qg), (k, kg), (v, vg))
+    for p in range(pairs):
+        for a, (source, target) in enumerate(arrays):
+            local_copies[p, a] = pltpu.make_async_copy(
+                source.at[:, pl.ds(pl.multiple_of(me * group + p * LANES, LANES), LANES)],
+                target.at[p, pl.ds(pl.multiple_of(me * tokens, tokens), tokens), :],
+                qkv_local.at[p, a])
+    pl.semaphore_wait(barrier, sp + 1)
+
+    qkv_copies = {}
+    order = [2, 1, 3] if sp == 4 else list(range(1, sp))
+
+    def send_pair(p):
+        for a, (source, target) in enumerate(arrays):
+            for d in order:
+                peer = lax.rem(me + d, sp)
+                copy = pltpu.make_async_remote_copy(
+                    src_ref=source.at[:, pl.ds(pl.multiple_of(peer * group + p * LANES, LANES), LANES)],
+                    dst_ref=target.at[p, pl.ds(pl.multiple_of(me * tokens, tokens), tokens), :],
+                    send_sem=qkv_send.at[p, a, d - 1],
+                    recv_sem=qkv_recv.at[p, a, d - 1],
+                    device_id=(peer, mine),
+                    device_id_type=MESH,
+                )
+                copy.start()
+                qkv_copies[p, a, d] = copy
+
+    ring_copies = {}
+    pair_copies = {}
+
+    def ring_slice(owner, side, step):
+        if step < steps - 1:
+            return wg.at[owner, core]
+        if side == 0:
+            return wg.at[owner, core, pl.ds(0, cut)]
+        return wg.at[owner, core, pl.ds(cut, rows - cut)]
+
+    def start_ring(key, source, target, side, slot):
+        copy = pltpu.make_async_remote_copy(
+            src_ref=source, dst_ref=target,
+            send_sem=ring_send.at[side, slot], recv_sem=ring_recv.at[side, slot],
+            device_id=(me, right if side == 0 else left), device_id_type=MESH)
+        copy.start()
+        ring_copies[key] = copy
+
+    def ring_first():
+        for side in range(2):
+            start_ring((side, 0), w.at[pl.ds(pl.multiple_of(core * half_rows, half_rows), half_rows), pl.ds(0, main)],
+                       wg.at[mine, core, pl.ds(0, half_rows)], side, 0)
+            start_ring((side, steps), tail.at[core],
+                       wg.at[mine, core, pl.ds(half_rows, tail_rows)], side, steps)
+
+    def ring_step(step):
+        for side in range(2):
+            ring_copies[side, step].wait_recv()
+            if step == 0:
+                ring_copies[side, steps].wait_recv()
+            shift = dp - 1 - step if side == 0 else 1 + step
+            owner = ring_index(lax.rem(position + shift, dp), dp)
+            if step + 1 < steps:
+                piece = ring_slice(owner, side, step + 1)
+                start_ring((side, step + 1), piece, piece, side, step + 1)
+            piece = ring_slice(owner, side, step)
+            copy = pltpu.make_async_remote_copy(
+                src_ref=piece, dst_ref=piece,
+                send_sem=pair_send.at[side, step], recv_sem=pair_recv.at[side, step],
+                device_id=(partner, mine), device_id_type=MESH)
+            copy.start()
+            pair_copies[side, step] = copy
+
+    send_pair(0)
+    ring_first()
+    for p in range(1, pairs):
+        send_pair(p)
+    for copy in local_copies.values():
+        copy.start()
+    for copy in own_copies:
+        copy.start()
+
+    log2e = math.log2(math.e)
+    factor = depth ** -0.5 * log2e
+    gates = gate[...] * log2e
+    gates_t = jnp.transpose(gates)
+    lane = lax.broadcasted_iota(jnp.int32, (tokens, LANES), 1) // depth
+    diagonal = (
+        lax.broadcasted_iota(jnp.int32, (tokens, tokens), 1)
+        <= lax.broadcasted_iota(jnp.int32, (tokens, tokens), 0)
+    )
+
+    def attend_block(p, i):
+        keys = (i + 1) * tokens
+        query = qg[p, i * tokens:keys, :]
+        key = kg[p, 0:keys, :]
+        value = vg[p, 0:keys, :]
+        result = jnp.zeros((tokens, LANES), jnp.float32)
+        for j in range(per_pair):
+            h = p * per_pair + j
+            masked = jnp.where(lane == j, query, jnp.zeros_like(query))
+            logits = lax.dot_general(
+                masked, key, (((1,), (1,)), ((), ())), preferred_element_type=jnp.float32
+            ) * factor
+            logits = logits + (gates_t[i * tokens:keys, h:h + 1] - gates[h:h + 1, 0:keys])
+            last = jnp.where(diagonal, logits[:, i * tokens:], -jnp.inf)
+            logits = jnp.concatenate([logits[:, :i * tokens], last], axis=1) if i else last
+            top = jnp.max(logits, axis=1, keepdims=True)
+            scores = jnp.exp2(logits - top)
+            total = jnp.sum(scores, axis=1, keepdims=True)
+            weighted = jnp.dot(scores.astype(jnp.bfloat16), value, preferred_element_type=jnp.float32)
+            result = jnp.where(lane == j, weighted / total, result)
+        og[p, i * tokens:keys, :] = result.astype(jnp.bfloat16)
+
+    out_copies = []
+
+    def send_out(p):
+        for d in order:
+            peer = lax.rem(me + d, sp)
+            copy = pltpu.make_async_remote_copy(
+                src_ref=og.at[p, pl.ds(pl.multiple_of(peer * tokens, tokens), tokens), :],
+                dst_ref=attended.at[:, pl.ds(pl.multiple_of(me * group + p * LANES, LANES), LANES)],
+                send_sem=out_send.at[p, d - 1], recv_sem=out_recv.at[p, d - 1],
+                device_id=(peer, mine), device_id_type=MESH)
+            copy.start()
+            out_copies.append(copy)
+        copy = pltpu.make_async_copy(
+            og.at[p, pl.ds(pl.multiple_of(me * tokens, tokens), tokens), :],
+            attended.at[:, pl.ds(pl.multiple_of(me * group + p * LANES, LANES), LANES)],
+            out_local.at[p])
+        copy.start()
+        own_copies.append(copy)
+
+    done = 0
+    for p in range(pairs):
+        if done < steps:
+            ring_step(done)
+            done += 1
+        for a in range(3):
+            local_copies[p, a].wait()
+            for d in order:
+                qkv_copies[p, a, d].wait_recv()
+        for i in range(sp):
+            if i == sp // 2 and p == pairs - 1 and done < steps:
+                ring_step(done)
+                done += 1
+            attend_block(p, i)
+        send_out(p)
+    while done < steps:
+        ring_step(done)
+        done += 1
+
+    for copy in own_copies:
+        copy.wait()
+    for copy in out_copies:
+        copy.wait()
+    for copy in pair_copies.values():
+        copy.wait()
+
+    tail_first = jnp.zeros((tokens, dp * tail_rows), jnp.float32)
+    tail_second = jnp.zeros((tokens, dp * tail_rows), jnp.float32)
+    quarter = half_rows // 2
+    nt = (((1,), (1,)), ((), ()))
+    for half in range(2):
+        packed = wg[:, half, half_rows:, :].reshape(dp * tail_rows, main)
+        tail_first += lax.dot_general(
+            attended[:, half * half_rows:half * half_rows + quarter], packed, nt,
+            preferred_element_type=jnp.float32)
+        tail_second += lax.dot_general(
+            attended[:, half * half_rows + quarter:(half + 1) * half_rows], packed, nt,
+            preferred_element_type=jnp.float32)
+    for owner in range(dp):
+        product = jnp.dot(
+            attended[:, :half_rows], wg[owner, 0, :half_rows, :], preferred_element_type=jnp.float32)
+        product += jnp.dot(
+            attended[:, half_rows:], wg[owner, 1, :half_rows, :], preferred_element_type=jnp.float32)
+        first = owner * tail_rows
+        second = first + tail_columns
+        end = (
+            tail_first[:, first:first + tail_columns]
+            + tail_second[:, second:second + tail_columns]
+        )
+        whole = jnp.concatenate([product, end], axis=1).astype(jnp.bfloat16)
+        out[:, owner * columns:(owner + 1) * columns] = whole
+
+    for copy in qkv_copies.values():
+        copy.wait_send()
+    for copy in ring_copies.values():
+        copy.wait_send()
+
+
+def fused(sp, dp, depth, q, k, v, gate, w):
+    tokens, width = q.shape
+    length = tokens * sp
+    columns = w.shape[1]
+    main = columns // LANES * LANES
+    half = width // 2
+    tail = w[:, main:].reshape(2, 2, half // 2, columns - main)
+    tail = tail.transpose(0, 1, 3, 2).reshape(2, 2 * (columns - main), main)
+    group = width // sp
+    pairs = group // LANES
+    steps = dp // 2
+    any_spec = pl.BlockSpec(memory_space=pl.ANY)
+    vmem_spec = pl.BlockSpec(memory_space=pltpu.VMEM)
+    dma = pltpu.SemaphoreType.DMA
+    gathered = pltpu.VMEM((pairs, length, LANES), jnp.bfloat16)
+    return pl.pallas_call(
+        functools.partial(fused_kernel, sp, dp, depth),
+        out_shape=jax.ShapeDtypeStruct((tokens, columns * dp), jnp.bfloat16),
+        in_specs=[any_spec, any_spec, any_spec, vmem_spec, any_spec, vmem_spec],
+        out_specs=vmem_spec,
+        scratch_shapes=[
+            gathered, gathered, gathered, gathered,
+            pltpu.VMEM((tokens, width), jnp.bfloat16),
+            pltpu.VMEM((dp, 2, half + tail.shape[1], main), jnp.bfloat16),
+            dma((pairs, 3, sp - 1)), dma((pairs, 3, sp - 1)), dma((pairs, 3)),
+            dma((pairs, sp - 1)), dma((pairs, sp - 1)), dma((pairs,)),
+            dma((2, steps + 1)), dma((2, steps + 1)),
+            dma((2, steps)), dma((2, steps)), dma((4,)),
+        ],
+        compiler_params=pltpu.CompilerParams(
+            collective_id=0, has_side_effects=True, vmem_limit_bytes=48 * 1024 * 1024),
+    )(q, k, v, gate, w, tail)
+
+
+def fits(sp, dp, tokens, width, depth, columns):
+    main = columns // LANES * LANES
+    return (
+        sp % 2 == 0 and dp % 2 == 0 and dp >= 4
+        and (width // sp) % LANES == 0 and LANES % depth == 0
+        and tokens * sp <= 1024 and tokens % LANES == 0
+        and main * 4 == width and columns > main
+        and 2 * (columns - main) == SUBLANES
+    )
 
 
 def attend(query_all, key_all, value_all, gate_all):
@@ -61,6 +352,12 @@
 
 
 def body(queries, keys, values, cum_gate, out_weight):
+    sp, dp = lax.axis_size("sp"), lax.axis_size("dp")
+    tokens, width = queries.shape[1:]
+    depth = width // (cum_gate.shape[1] * sp)
+    if fits(sp, dp, tokens, width, depth, out_weight.shape[1]):
+        mixed = fused(sp, dp, depth, queries[0], keys[0], values[0], cum_gate[0], out_weight)
+        return mixed[None]
     query_heads, key_heads, value_heads = (
         lax.all_to_all(queries, "sp", split_axis=2, concat_axis=1, tiled=True),
         lax.all_to_all(keys, "sp", split_axis=2, concat_axis=1, tiled=True),

time: 111 us -> 39.5 us (0.36)
  Pallas kernels: 0 us -> 34.6 us
  other arithmetic: 20.1 us -> 0 us
  local copies, waits for them, and re-layouts: 21.2 us -> 4.61 us
  between operations: 13.7 us -> 0.05 us
  blocking collectives: 13.2 us -> 0 us
  matrix products: 13 us -> 0 us
  starting transfers between devices: 12.1 us -> 0 us
  waiting for transfers between devices: 10.6 us -> 0 us
  loops' own time: 6.82 us -> 0 us
    pallas_call x0 -> x1, Pallas kernels: none -> 34.6 us  [fused(): pl.pallas_call(functools.partial(fused_kernel, sp, dp, depth), out_shape=...]
    unnamed x4 -> x0, other arithmetic: 15.2 us -> none
    all_to_all x1 -> x0, blocking collectives: 13.2 us -> none  [body(): lax.all_to_all(local_out[None], 'sp', split_axis=1, concat_axis=2, tiled=...]
    dot_general x7 -> x0, matrix products: 13 us -> none  [the longest x3 4.72 us: key_step(): jnp.einsum('hqk,khe->hqe', scores.astype(jnp.bfloat16), value_part, prefe...]
    unnamed x27 -> x9, local copies, waits for them, and re-layouts: 15.3 us -> 2.45 us
    all_to_all x3 -> x0, starting transfers between devices: 11.9 us -> none  [the longest x1 4.26 us: body(): lax.all_to_all(queries, 'sp', split_axis=2, concat_axis=1, tiled=True)]
    all_to_all x3 -> x0, waiting for transfers between devices: 10.6 us -> none  [the longest x1 5.69 us: body(): lax.all_to_all(values, 'sp', split_axis=2, concat_axis=1, tiled=True)]
    another operation x3 -> x0, loops' own time: 6.82 us -> none  [the longest x1 6.51 us: attend(): outputs = lax.map(one_block, jnp.arange(block_count, dtype=jnp.int32))]
  transfers between devices with their start and end apart: 5 -> 0, of which waited for: 3 -> 0; matrix products, arithmetic and copies ran while one was open for 43% -> 0% of each run, Pallas kernels for 0% -> 0%
where the time goes in v1:
time: 39.5 us; the launch traced here: 39.2 us
  Pallas kernels  34.6 us (88%)
  local copies, waits for them, and re-layouts  4.61 us (12%)
    pallas_call x1, Pallas kernels, fused(): pl.pallas_call(functools.partial(fused_kernel, sp, dp, depth), out_shape=...  34.6 us
    unnamed x9, local copies, waits for them, and re-layouts  2.45 us
    broadcast_in_dim x1, local copies, waits for them, and re-layouts, body(): return mixed[None]  1.35 us
    slice x1, local copies, waits for them, and re-layouts, fused(): tail = w[:, main:].reshape(2, 2, half // 2, columns - main)  0.81 us

profile of v1, /device:TPU:0, one launch (start us, length us, event | category | flops | bytes accessed | tf_op | source)
XLA Modules:
  0.0 39.2 jit_solution(3896398497616375754)
XLA Ops:
  0.0 0.0 copy-start.3
  0.0 0.0 copy-start.1
  0.0 0.0 copy-start
  0.0 0.8 %slice.3 = bf16[1024,8]{0,1:T(8,128)(2,1)S(1)} slice(bf16[1024,264]{0,1:T(8,128)(2,1)} %param.9), slice={[0:1024], [256:264]} | slice | bytes 32768 | tf_op jit(solution)/shard_map/slice | solution.py:259
  0.8 1.4 %copy.6.w = bf16[1024,264]{1,0:T(8,128)(2,1)S(1)} copy(bf16[1024,264]{0,1:T(8,128)(2,1)} %param.9) | data formatting | bytes 1081344 | tf_op args[4]
  2.2 0.0 copy-done.3
  2.2 0.0 copy-done.1
  2.2 0.0 copy-done
  2.3 0.0 copy-start.2
  2.3 1.0 %copy-done.2 = bf16[1,256,1024]{2,1,0:T(8,128)(2,1)S(1)} copy-done((bf16[1,256,1024]{2,1,0:T(8,128)(2,1)S(1)}, bf16[1,256,1024]{2,1,0:T(8,128)(2,1)}, u32[]{:S(2)}) %copy-start.2) | copy-done | bytes 524312
  3.3 34.6 %shard_map.55 = bf16[256,2112]{1,0:T(8,128)(2,1)S(1)} custom-call(bf16[256,1024]{1,0:T(8,128)(2,1)S(1)} %bitcast.11, bf16[256,1024]{1,0:T(8,128)(2,1)S(1)} %bitcast.12, bf16[256,1024]{1,0:T(8,128)(2,1)S(1)} %bitcast.13, f32[4,1024]{1,0:T(4,128)S(1)} %bitcast.15, bf16[1024,264]{1,0:T(8,128)(2,1)S(1)} %copy.6.w, bf16[2,16,256]{2,1,0:T(8,128)(2,1)S(1)} %bitcast.14), custom_call_target="tpu_custom_call" | custom-call | tf_op jit(solution)/shard_map/pallas_call | solution.py:268
  37.9 1.4 %copy.7 = bf16[1,256,2112]{1,2,0:T(8,128)(2,1)} copy(bf16[1,256,2112]{2,1,0:T(8,128)(2,1)S(1)} %bitcast.10) | data formatting | bytes 2162688 | tf_op jit(solution)/shard_map/broadcast_in_dim | solution.py:360
Async XLA Ops:
  0.0 2.2 %copy-start.3 = (f32[1,4,1024]{2,1,0:T(4,128)S(1)}, f32[1,4,1024]{2,1,0:T(4,128)}, u32[]{:S(2)}) copy-start(f32[1,4,1024]{2,1,0:T(4,128)} %param.8) | copy-start | bytes 49156
  0.0 2.2 %copy-start.1 = (bf16[1,256,1024]{2,1,0:T(8,128)(2,1)S(1)}, bf16[1,256,1024]{2,1,0:T(8,128)(2,1)}, u32[]{:S(2)}) copy-start(bf16[1,256,1024]{2,1,0:T(8,128)(2,1)} %param.6) | copy-start | bytes 1572868
  0.0 2.2 %copy-start = (bf16[1,256,1024]{2,1,0:T(8,128)(2,1)S(1)}, bf16[1,256,1024]{2,1,0:T(8,128)(2,1)}, u32[]{:S(2)}) copy-start(bf16[1,256,1024]{2,1,0:T(8,128)(2,1)} %param.5) | copy-start | bytes 1572868
  2.3 1.0 %copy-start.2 = (bf16[1,256,1024]{2,1,0:T(8,128)(2,1)S(1)}, bf16[1,256,1024]{2,1,0:T(8,128)(2,1)}, u32[]{:S(2)}) copy-start(bf16[1,256,1024]{2,1,0:T(8,128)(2,1)} %param.7) | copy-start | bytes 1572868

commit v2 on v0

--- a/solution.py
+++ b/solution.py
@@ -1,7 +1,423 @@
+import functools
+import math
+
 import jax
 import jax.numpy as jnp
 from jax import lax
+from jax.experimental import pallas as pl
+from jax.experimental.pallas import tpu as pltpu
 from jax.sharding import PartitionSpec as P
+
+LANES = 128
+SUBLANES = 16
+MESH = pl.DeviceIdType.MESH
+
+
+def ring_index(position, n):
+    upper = position // (n // 2)
+    return (1 - upper) * (2 * position) + upper * (2 * (n - 1 - position) + 1)
+
+
+def fused_kernel(
+    dp, depth, q, k, v, gate, w, out,
+    qg, kg, vg, qx, local_f32, local_stats, ox, orx, sx, srx, done_out, attended, gates_all, wfull, wg,
+    gate_send, gate_recv, swap_send, swap_recv, swap_local, qx_send, qx_recv,
+    ox_send, ox_recv, sx_send, sx_recv, fin_send, fin_recv, fin_local,
+    ring_send, ring_recv, pair_send, pair_recv, own_sem,
+):
+    tokens, width = q.shape
+    group = width // 2
+    chip_rows = 2 * tokens
+    pairs = group // LANES
+    per_pair = LANES // depth
+    half_rows = width // 2
+    main = wg.shape[3]
+    rows = wg.shape[2]
+    tail_rows = rows - half_rows
+    columns = w.shape[1]
+    tail_columns = columns - main
+    steps = dp // 2
+    cut = -(-(rows // 2) // SUBLANES) * SUBLANES
+    me = lax.axis_index("sp")
+    mine = lax.axis_index("dp")
+    core = lax.rem(me, 2)
+    chip = me // 2
+    partner = me + 1 - 2 * core
+    odd = lax.rem(mine, 2)
+    position = (1 - odd) * (mine // 2) + odd * (dp - 1 - mine // 2)
+    right = ring_index(lax.rem(position + 1, dp), dp)
+    left = ring_index(lax.rem(position + dp - 1, dp), dp)
+
+    def remote(source, target, send, recv, sp_index, dp_index):
+        return pltpu.make_async_remote_copy(
+            src_ref=source, dst_ref=target, send_sem=send, recv_sem=recv,
+            device_id=(sp_index, dp_index), device_id_type=MESH)
+
+    def aligned(index, size):
+        return pl.ds(pl.multiple_of(index * size, size), size)
+
+    barrier = pltpu.get_barrier_semaphore()
+    for d in range(1, 4):
+        pl.semaphore_signal(
+            barrier, inc=1, device_id=(lax.rem(me + d, 4), mine), device_id_type=MESH
+        )
+    for side in (left, right):
+        pl.semaphore_signal(barrier, inc=1, device_id=(me, side), device_id_type=MESH)
+
+    whole_w = pltpu.make_async_copy(w, wfull, own_sem.at[0])
+    whole_w.start()
+    own_copies = [
+        pltpu.make_async_copy(
+            w.at[pl.ds(half * half_rows, half_rows), pl.ds(0, main)],
+            wg.at[mine, half, pl.ds(0, half_rows)], own_sem.at[1 + half])
+        for half in range(2)
+    ]
+    arrays = ((q, qg), (k, kg), (v, vg))
+    swap_copies, local_copies = [], []
+    for a, (source, target) in enumerate(arrays):
+        swap_copies.append(remote(
+            source.at[:, aligned(1 - core, group)], target.at[aligned(core, tokens), :],
+            swap_send.at[a], swap_recv.at[a], partner, mine))
+        local_copies.append(pltpu.make_async_copy(
+            source.at[:, aligned(core, group)], target.at[aligned(core, tokens), :], swap_local.at[a]))
+    gate_copies = [
+        remote(gate, gates_all.at[me], gate_send.at[d - 1], gate_recv.at[d - 1],
+               lax.rem(me + d, 4), mine)
+        for d in range(1, 4)
+    ]
+    query_sends = {
+        (p, a): remote(
+            q.at[:, pl.ds(a * group + p * LANES, LANES)],
+            qx.at[aligned(core, tokens), pl.ds(p * LANES, LANES)],
+            qx_send.at[p, a], qx_recv.at[p, core], a, mine)
+        for p in range(pairs) for a in range(2)
+    }
+    query_recvs = {
+        (p, c): remote(
+            q.at[:, pl.ds(p * LANES, LANES)],
+            qx.at[pl.ds(c * tokens, tokens), pl.ds(p * LANES, LANES)],
+            qx_send.at[p, c], qx_recv.at[p, c], partner, mine)
+        for p in range(pairs) for c in range(2)
+    }
+    across = lax.rem(me + 2, 4)
+    cross_sends = {
+        (p, i): remote(
+            ox.at[pl.ds(i * tokens, tokens), pl.ds(p * LANES, LANES)],
+            orx.at[pl.ds(i * tokens, tokens), pl.ds(p * LANES, LANES)],
+            ox_send.at[p, i], ox_recv.at[p, i], across, mine)
+        for p in range(pairs) for i in range(2)
+    }
+    stat_sends = {
+        (p, i): remote(sx.at[p, i], srx.at[p, i], sx_send.at[p, i], sx_recv.at[p, i], across, mine)
+        for p in range(pairs) for i in range(2)
+    }
+    final_copy = remote(
+        done_out.at[aligned(1 - core, tokens), :], attended.at[:, aligned(core, group)],
+        fin_send.at[0], fin_recv.at[0], partner, mine)
+    final_local = pltpu.make_async_copy(
+        done_out.at[aligned(core, tokens), :], attended.at[:, aligned(core, group)], fin_local.at[0])
+
+    spans = ((0, cut), (cut, rows - cut))
+    ring, swap_weight = {}, {}
+    for side in range(2):
+        target = right if side == 0 else left
+        for step in range(steps):
+            shift = lax.rem(position + (dp - step if side == 0 else step), dp)
+            sent = ring_index(shift, dp)
+            shift = lax.rem(position + (dp - 1 - step if side == 0 else 1 + step), dp)
+            came = ring_index(shift, dp)
+            for piece, (start, size) in enumerate(spans):
+                if step == steps - 1 and piece != side:
+                    continue
+                span = pl.ds(start, size)
+                source = wg.at[sent, core, span]
+                if step == 0:
+                    if piece == 1:
+                        span = pl.ds(start, size - tail_rows)
+                        size -= tail_rows
+                    source = w.at[pl.ds(pl.multiple_of(core * half_rows + start, SUBLANES), size), pl.ds(0, main)]
+                ring[side, step, piece] = remote(
+                    source, wg.at[sent, core, span],
+                    ring_send.at[side, step, piece], ring_recv.at[side, step, piece], me, target)
+                span = pl.ds(start, spans[piece][1])
+                swap_weight[side, step, piece] = remote(
+                    wg.at[came, core, span], wg.at[came, core, span],
+                    pair_send.at[side, step, piece], pair_recv.at[side, step, piece], partner, mine)
+        span = pl.ds(half_rows, tail_rows)
+        ring[side, "tail"] = remote(
+            wg.at[mine, core, span], wg.at[mine, core, span],
+            ring_send.at[side, steps, 0], ring_recv.at[side, steps, 0], me, target)
+
+    events = [(step, piece) for step in range(steps - 1) for piece in range(2)]
+
+    def ring_event(n):
+        if n < len(events):
+            step, piece = events[n]
+            for side in range(2):
+                ring[side, step, piece].wait_recv()
+                if step == 0 and piece == 1:
+                    ring[side, "tail"].wait_recv()
+                if (side, step + 1, piece) in ring:
+                    ring[side, step + 1, piece].start()
+                swap_weight[side, step, piece].start()
+        elif n == len(events):
+            for side in range(2):
+                ring[side, steps - 1, side].wait_recv()
+                swap_weight[side, steps - 1, side].start()
+
+    pl.semaphore_wait(barrier, 5)
+    for copy in gate_copies + swap_copies:
+        copy.start()
+
+    @pl.when(chip == 1)
+    def _():
+        for p in range(pairs):
+            for a in range(2):
+                query_sends[p, a].start()
+
+    for piece in range(2):
+        for side in range(2):
+            ring[side, 0, piece].start()
+    for copy in local_copies + own_copies:
+        copy.start()
+    gates_all[me] = gate[...]
+
+    whole_w.wait()
+    quarter = half_rows // 2
+    nt = (((1,), (1,)), ((), ()))
+    picked = lax.broadcasted_iota(jnp.int32, (tail_rows, tail_columns), 0)
+    column = lax.broadcasted_iota(jnp.int32, (tail_rows, tail_columns), 1)
+    for half in range(2):
+        packed = jnp.zeros((tail_rows, quarter), jnp.float32)
+        for a in range(2):
+            chosen = jnp.where(picked == column + a * tail_columns, 1.0, 0.0).astype(jnp.bfloat16)
+            first = half * half_rows + a * quarter
+            packed += lax.dot_general(
+                chosen, wfull[first:first + quarter, main:], nt, preferred_element_type=jnp.float32)
+        wg[mine, half, half_rows:, :] = packed.astype(jnp.bfloat16)
+    for side in range(2):
+        ring[side, "tail"].start()
+
+    log2e = math.log2(math.e)
+    factor = depth ** -0.5 * log2e
+    lane = lax.broadcasted_iota(jnp.int32, (tokens, LANES), 1)
+    head_lane = lane // depth
+    diagonal = (
+        lax.broadcasted_iota(jnp.int32, (tokens, tokens), 1)
+        <= lax.broadcasted_iota(jnp.int32, (tokens, tokens), 0)
+    )
+    heads_held = gates_all.shape[1]
+
+    def block(p, query, keys, causal, query_first, key_first):
+        key = kg[0:keys, p * LANES:(p + 1) * LANES]
+        value = vg[0:keys, p * LANES:(p + 1) * LANES]
+        holder = core * 2 + p * per_pair // heads_held
+        query_gates = jnp.transpose(gates_all[holder, :, query_first:query_first + tokens]) * log2e
+        key_gates = gates_all[holder, :, key_first:key_first + keys] * log2e
+        parts = []
+        for j in range(per_pair):
+            h = p * per_pair % heads_held + j
+            masked = jnp.where(head_lane == j, query, jnp.zeros_like(query))
+            logits = lax.dot_general(masked, key, nt, preferred_element_type=jnp.float32) * factor
+            logits = logits + (query_gates[:, h:h + 1] - key_gates[h:h + 1, :])
+            if causal:
+                last = jnp.where(diagonal, logits[:, keys - tokens:], -jnp.inf)
+                logits = jnp.concatenate([logits[:, :keys - tokens], last], axis=1) if keys > tokens else last
+            top = jnp.max(logits, axis=1, keepdims=True)
+            scores = jnp.exp2(logits - top)
+            total = jnp.sum(scores, axis=1, keepdims=True)
+            weighted = jnp.dot(scores.astype(jnp.bfloat16), value, preferred_element_type=jnp.float32)
+            parts.append((weighted, top, total))
+        return parts
+
+    def by_head(values):
+        result = values[0]
+        for j in range(1, per_pair):
+            result = jnp.where(head_lane == j, values[j], result)
+        return result
+
+    def stats_of(parts):
+        result = jnp.zeros((tokens, LANES), jnp.float32)
+        for j, (_, top, total) in enumerate(parts):
+            result = jnp.where(lane == j, top, result)
+            result = jnp.where(lane == per_pair + j, total, result)
+        return result
+
+    def wait_swapped():
+        for copy in local_copies:
+            copy.wait()
+        for copy in swap_copies + gate_copies:
+            copy.wait_recv()
+
+    def pair_columns(p):
+        return slice(p * LANES, (p + 1) * LANES)
+
+    @pl.when(chip == 0)
+    def _():
+        wait_swapped()
+        for p in range(pairs):
+            for i in range(2):
+                first = i * tokens
+                parts = block(p, qg[first:first + tokens, pair_columns(p)], first + tokens, True, first, 0)
+                done_out[first:first + tokens, pair_columns(p)] = by_head(
+                    [weighted / total for weighted, _, total in parts]).astype(jnp.bfloat16)
+            if p == pairs // 2 - 1:
+                ring_event(0)
+        final_copy.start()
+        final_local.start()
+        ring_event(1)
+        for p in range(pairs):
+            if p == pairs // 2:
+                ring_event(2)
+            for c in range(2):
+                query_recvs[p, c].wait_recv()
+            for i in range(2):
+                first = i * tokens
+                parts = block(
+                    p, qx[first:first + tokens, pair_columns(p)], chip_rows, False, chip_rows + first, 0)
+                ox[first:first + tokens, pair_columns(p)] = by_head(
+                    [weighted / total for weighted, _, total in parts]).astype(jnp.bfloat16)
+                sx[p, i] = jnp.transpose(stats_of(parts))[:8, :]
+                cross_sends[p, i].start()
+                stat_sends[p, i].start()
+        ring_event(3)
+        ring_event(4)
+        for copy in list(cross_sends.values()) + list(stat_sends.values()):
+            copy.wait_send()
+
+    @pl.when(chip == 1)
+    def _():
+        wait_swapped()
+        for p in range(pairs):
+            for i in range(2):
+                first = i * tokens
+                parts = block(
+                    p, qg[first:first + tokens, pair_columns(p)], first + tokens, True,
+                    chip_rows + first, chip_rows)
+                local_f32[first:first + tokens, pair_columns(p)] = by_head([part[0] for part in parts])
+                local_stats[p, first:first + tokens, :] = stats_of(parts)
+            if p == pairs // 2 - 1:
+                ring_event(0)
+        ring_event(1)
+        for p in range(pairs):
+            if p == 1:
+                ring_event(2)
+            if p == 2:
+                ring_event(3)
+            if p == 3:
+                ring_event(4)
+            for i in range(2):
+                first = i * tokens
+                cross_sends[p, i].wait_recv()
+                stat_sends[p, i].wait_recv()
+                far_stats = jnp.transpose(srx[p, i])
+                near_stats = local_stats[p, first:first + tokens, :]
+                near, far, total = [], [], []
+                for j in range(per_pair):
+                    near_top, far_top = near_stats[:, j:j + 1], far_stats[:, j:j + 1]
+                    top = jnp.maximum(near_top, far_top)
+                    near_factor = jnp.exp2(near_top - top)
+                    far_factor = jnp.exp2(far_top - top) * far_stats[:, per_pair + j:per_pair + j + 1]
+                    total = near_factor * near_stats[:, per_pair + j:per_pair + j + 1] + far_factor
+                    near.append(near_factor / total)
+                    far.append(far_factor / total)
+                merged = (
+                    local_f32[first:first + tokens, pair_columns(p)] * by_head(near)
+                    + orx[first:first + tokens, pair_columns(p)].astype(jnp.float32) * by_head(far)
+                )
+                done_out[first:first + tokens, pair_columns(p)] = merged.astype(jnp.bfloat16)
+        final_copy.start()
+        final_local.start()
+        for copy in query_sends.values():
+            copy.wait_send()
+
+    for n in range(5, len(events) + 1):
+        ring_event(n)
+
+    for copy in own_copies:
+        copy.wait()
+    final_local.wait()
+    final_copy.wait()
+    for copy in swap_weight.values():
+        copy.wait()
+
+    tail_first = jnp.zeros((tokens, dp * tail_rows), jnp.float32)
+    tail_second = jnp.zeros((tokens, dp * tail_rows), jnp.float32)
+    for half in range(2):
+        packed = wg[:, half, half_rows:, :].reshape(dp * tail_rows, main)
+        tail_first += lax.dot_general(
+            attended[:, half * half_rows:half * half_rows + quarter], packed, nt,
+            preferred_element_type=jnp.float32)
+        tail_second += lax.dot_general(
+            attended[:, half * half_rows + quarter:(half + 1) * half_rows], packed, nt,
+            preferred_element_type=jnp.float32)
+    for owner in range(dp):
+        product = jnp.dot(
+            attended[:, :half_rows], wg[owner, 0, :half_rows, :], preferred_element_type=jnp.float32)
+        product += jnp.dot(
+            attended[:, half_rows:], wg[owner, 1, :half_rows, :], preferred_element_type=jnp.float32)
+        first = owner * tail_rows
+        second = first + tail_columns
+        end = (
+            tail_first[:, first:first + tail_columns]
+            + tail_second[:, second:second + tail_columns]
+        )
+        whole = jnp.concatenate([product, end], axis=1).astype(jnp.bfloat16)
+        out[:, owner * columns:(owner + 1) * columns] = whole
+
+    for copy in gate_copies + swap_copies + list(ring.values()):
+        copy.wait_send()
+
+
+def fused(dp, depth, q, k, v, gate, w):
+    tokens, width = q.shape
+    columns = w.shape[1]
+    main = columns // LANES * LANES
+    half = width // 2
+    pairs = half // LANES
+    steps = dp // 2
+    any_spec = pl.BlockSpec(memory_space=pl.ANY)
+    vmem_spec = pl.BlockSpec(memory_space=pltpu.VMEM)
+    dma = pltpu.SemaphoreType.DMA
+    held = pltpu.VMEM((2 * tokens, half), jnp.bfloat16)
+    stats = pltpu.VMEM((pairs, 2, 8, tokens), jnp.float32)
+    return pl.pallas_call(
+        functools.partial(fused_kernel, dp, depth),
+        out_shape=jax.ShapeDtypeStruct((tokens, columns * dp), jnp.bfloat16),
+        in_specs=[any_spec, any_spec, any_spec, vmem_spec, any_spec],
+        out_specs=vmem_spec,
+        scratch_shapes=[
+            held, held, held, held,
+            pltpu.VMEM((2 * tokens, half), jnp.float32),
+            pltpu.VMEM((pairs, 2 * tokens, LANES), jnp.float32),
+            held, held, stats, stats, held,
+            pltpu.VMEM((tokens, width), jnp.bfloat16),
+            pltpu.VMEM((4,) + gate.shape, jnp.float32),
+            pltpu.VMEM(w.shape, jnp.bfloat16),
+            pltpu.VMEM((dp, 2, half + SUBLANES, main), jnp.bfloat16),
+            dma((3,)), dma((3,)), dma((3,)), dma((3,)), dma((3,)),
+            dma((pairs, 2)), dma((pairs, 2)),
+            dma((pairs, 2)), dma((pairs, 2)), dma((pairs, 2)), dma((pairs, 2)),
+            dma((1,)), dma((1,)), dma((1,)),
+            dma((2, steps + 1, 2)), dma((2, steps + 1, 2)),
+            dma((2, steps, 2)), dma((2, steps, 2)), dma((3,)),
+        ],
+        compiler_params=pltpu.CompilerParams(
+            collective_id=0, has_side_effects=True, vmem_limit_bytes=48 * 1024 * 1024),
+    )(q, k, v, gate, w)
+
+
+def fits(sp, dp, tokens, width, depth, columns):
+    main = columns // LANES * LANES
+    return (
+        sp == 4 and dp % 2 == 0 and 8 <= dp <= 16
+        and width % (2 * LANES) == 0 and width <= 1024 and LANES % depth == 0
+        and tokens <= 256 and tokens % LANES == 0
+        and (width // depth // sp) % (LANES // depth) == 0
+        and LANES // depth <= 4
+        and main * 4 == width and columns > main
+        and 2 * (columns - main) == SUBLANES
+    )
 
 
 def attend(query_all, key_all, value_all, gate_all):
@@ -61,6 +477,12 @@
 
 
 def body(queries, keys, values, cum_gate, out_weight):
+    sp, dp = lax.axis_size("sp"), lax.axis_size("dp")
+    tokens, width = queries.shape[1:]
+    depth = width // (cum_gate.shape[1] * sp)
+    if fits(sp, dp, tokens, width, depth, out_weight.shape[1]):
+        mixed = fused(dp, depth, queries[0], keys[0], values[0], cum_gate[0], out_weight)
+        return mixed[None]
     query_heads, key_heads, value_heads = (
         lax.all_to_all(queries, "sp", split_axis=2, concat_axis=1, tiled=True),
         lax.all_to_all(keys, "sp", split_axis=2, concat_axis=1, tiled=True),

time: 111 us -> 41.2 us (0.37)
  Pallas kernels: 0 us -> 36.5 us
  other arithmetic: 20.1 us -> 0 us
  local copies, waits for them, and re-layouts: 21.2 us -> 3.89 us
  between operations: 13.7 us -> 0.05 us
  blocking collectives: 13.2 us -> 0 us
  matrix products: 13 us -> 0 us
  starting transfers between devices: 12.1 us -> 0 us
  waiting for transfers between devices: 10.6 us -> 0 us
  loops' own time: 6.82 us -> 0 us
    pallas_call x0 -> x1, Pallas kernels: none -> 36.5 us  [fused(): pl.pallas_call(functools.partial(fused_kernel, dp, depth), out_shape=jax....]
    unnamed x4 -> x0, other arithmetic: 15.2 us -> none
    all_to_all x1 -> x0, blocking collectives: 13.2 us -> none  [body(): lax.all_to_all(local_out[None], 'sp', split_axis=1, concat_axis=2, tiled=...]
    dot_general x7 -> x0, matrix products: 13 us -> none  [the longest x3 4.72 us: key_step(): jnp.einsum('hqk,khe->hqe', scores.astype(jnp.bfloat16), value_part, prefe...]
    unnamed x27 -> x9, local copies, waits for them, and re-layouts: 15.3 us -> 2.54 us
    all_to_all x3 -> x0, starting transfers between devices: 11.9 us -> none  [the longest x1 4.26 us: body(): lax.all_to_all(queries, 'sp', split_axis=2, concat_axis=1, tiled=True)]
    all_to_all x3 -> x0, waiting for transfers between devices: 10.6 us -> none  [the longest x1 5.69 us: body(): lax.all_to_all(values, 'sp', split_axis=2, concat_axis=1, tiled=True)]
    another operation x3 -> x0, loops' own time: 6.82 us -> none  [the longest x1 6.51 us: attend(): outputs = lax.map(one_block, jnp.arange(block_count, dtype=jnp.int32))]
  transfers between devices with their start and end apart: 5 -> 0, of which waited for: 3 -> 0; matrix products, arithmetic and copies ran while one was open for 43% -> 0% of each run, Pallas kernels for 0% -> 0%
where the time goes in v2:
time: 41.2 us; the launch traced here: 40.5 us
  Pallas kernels  36.5 us (89%)
  local copies, waits for them, and re-layouts  3.89 us (9%)
    pallas_call x1, Pallas kernels, fused(): pl.pallas_call(functools.partial(fused_kernel, dp, depth), out_shape=jax....  36.5 us
    unnamed x9, local copies, waits for them, and re-layouts  2.54 us
    broadcast_in_dim x1, local copies, waits for them, and re-layouts, body(): return mixed[None]  1.35 us

profile of v2, /device:TPU:0, one launch (start us, length us, event | category | flops | bytes accessed | tf_op | source)
XLA Modules:
  0.0 40.5 jit_solution(11390511538523110577)
XLA Ops:
  0.0 0.0 copy-start.3
  0.0 0.0 copy-start.1
  0.0 0.0 copy-start
  0.0 1.5 %copy.6.w = bf16[1024,264]{1,0:T(8,128)(2,1)S(1)} copy(bf16[1024,264]{0,1:T(8,128)(2,1)} %param.9) | data formatting | bytes 1081344 | tf_op args[4]
  1.5 0.0 copy-done.3
  1.5 0.0 copy-done.1
  1.5 0.0 copy-done
  1.5 0.0 copy-start.2
  1.5 1.0 %copy-done.2 = bf16[1,256,1024]{2,1,0:T(8,128)(2,1)S(1)} copy-done((bf16[1,256,1024]{2,1,0:T(8,128)(2,1)S(1)}, bf16[1,256,1024]{2,1,0:T(8,128)(2,1)}, u32[]{:S(2)}) %copy-start.2) | copy-done | bytes 524312
  2.6 36.5 %shard_map.55 = bf16[256,2112]{1,0:T(8,128)(2,1)S(1)} custom-call(bf16[256,1024]{1,0:T(8,128)(2,1)S(1)} %bitcast.6, bf16[256,1024]{1,0:T(8,128)(2,1)S(1)} %bitcast.7, bf16[256,1024]{1,0:T(8,128)(2,1)S(1)} %bitcast.8, f32[4,1024]{1,0:T(4,128)S(1)} %bitcast.9, bf16[1024,264]{1,0:T(8,128)(2,1)S(1)} %copy.6.w), custom_call_target="tpu_custom_call" | custom-call | tf_op jit(solution)/shard_map/pallas_call | solution.py:384
  39.1 1.4 %copy.7 = bf16[1,256,2112]{1,2,0:T(8,128)(2,1)} copy(bf16[1,256,2112]{2,1,0:T(8,128)(2,1)S(1)} %bitcast.5) | data formatting | bytes 2162688 | tf_op jit(solution)/shard_map/broadcast_in_dim | solution.py:485
Async XLA Ops:
  0.0 1.5 %copy-start.3 = (f32[1,4,1024]{2,1,0:T(4,128)S(1)}, f32[1,4,1024]{2,1,0:T(4,128)}, u32[]{:S(2)}) copy-start(f32[1,4,1024]{2,1,0:T(4,128)} %param.8) | copy-start | bytes 49156
  0.0 1.5 %copy-start.1 = (bf16[1,256,1024]{2,1,0:T(8,128)(2,1)S(1)}, bf16[1,256,1024]{2,1,0:T(8,128)(2,1)}, u32[]{:S(2)}) copy-start(bf16[1,256,1024]{2,1,0:T(8,128)(2,1)} %param.6) | copy-start | bytes 1572868
  0.0 1.5 %copy-start = (bf16[1,256,1024]{2,1,0:T(8,128)(2,1)S(1)}, bf16[1,256,1024]{2,1,0:T(8,128)(2,1)}, u32[]{:S(2)}) copy-start(bf16[1,256,1024]{2,1,0:T(8,128)(2,1)} %param.5) | copy-start | bytes 1572868
  1.5 1.0 %copy-start.2 = (bf16[1,256,1024]{2,1,0:T(8,128)(2,1)S(1)}, bf16[1,256,1024]{2,1,0:T(8,128)(2,1)}, u32[]{:S(2)}) copy-start(bf16[1,256,1024]{2,1,0:T(8,128)(2,1)} %param.7) | copy-start | bytes 1572868

commit v3 on v2

--- a/solution.py
+++ b/solution.py
@@ -9,7 +9,6 @@
 from jax.sharding import PartitionSpec as P
 
 LANES = 128
-SUBLANES = 16
 MESH = pl.DeviceIdType.MESH
 
 
@@ -20,7 +19,7 @@
 
 def fused_kernel(
     dp, depth, q, k, v, gate, w, out,
-    qg, kg, vg, qx, local_f32, local_stats, ox, orx, sx, srx, done_out, attended, gates_all, wfull, wg,
+    qg, kg, vg, qx, local_f32, local_stats, ox, orx, sx, srx, done_out, attended, gates_all, wg,
     gate_send, gate_recv, swap_send, swap_recv, swap_local, qx_send, qx_recv,
     ox_send, ox_recv, sx_send, sx_recv, fin_send, fin_recv, fin_local,
     ring_send, ring_recv, pair_send, pair_recv, own_sem,
@@ -30,14 +29,9 @@
     chip_rows = 2 * tokens
     pairs = group // LANES
     per_pair = LANES // depth
-    half_rows = width // 2
-    main = wg.shape[3]
-    rows = wg.shape[2]
-    tail_rows = rows - half_rows
-    columns = w.shape[1]
-    tail_columns = columns - main
+    quarter = width // 4
+    columns = w.shape[0]
     steps = dp // 2
-    cut = -(-(rows // 2) // SUBLANES) * SUBLANES
     me = lax.axis_index("sp")
     mine = lax.axis_index("dp")
     core = lax.rem(me, 2)
@@ -64,13 +58,9 @@
     for side in (left, right):
         pl.semaphore_signal(barrier, inc=1, device_id=(me, side), device_id_type=MESH)
 
-    whole_w = pltpu.make_async_copy(w, wfull, own_sem.at[0])
-    whole_w.start()
     own_copies = [
-        pltpu.make_async_copy(
-            w.at[pl.ds(half * half_rows, half_rows), pl.ds(0, main)],
-            wg.at[mine, half, pl.ds(0, half_rows)], own_sem.at[1 + half])
-        for half in range(2)
+        pltpu.make_async_copy(w.at[:, pl.ds(n * quarter, quarter)], wg.at[mine, n], own_sem.at[n])
+        for n in range(4)
     ]
     arrays = ((q, qg), (k, kg), (v, vg))
     swap_copies, local_copies = [], []
@@ -117,8 +107,7 @@
     final_local = pltpu.make_async_copy(
         done_out.at[aligned(core, tokens), :], attended.at[:, aligned(core, group)], fin_local.at[0])
 
-    spans = ((0, cut), (cut, rows - cut))
-    ring, swap_weight = {}, {}
+    ring, swap_weight, came_from = {}, {}, {}
     for side in range(2):
         target = right if side == 0 else left
         for step in range(steps):
@@ -126,27 +115,18 @@
             sent = ring_index(shift, dp)
             shift = lax.rem(position + (dp - 1 - step if side == 0 else 1 + step), dp)
             came = ring_index(shift, dp)
-            for piece, (start, size) in enumerate(spans):
+            came_from[side, step] = came
+            for piece in range(2):
                 if step == steps - 1 and piece != side:
                     continue
-                span = pl.ds(start, size)
-                source = wg.at[sent, core, span]
-                if step == 0:
-                    if piece == 1:
-                        span = pl.ds(start, size - tail_rows)
-                        size -= tail_rows
-                    source = w.at[pl.ds(pl.multiple_of(core * half_rows + start, SUBLANES), size), pl.ds(0, main)]
+                place = 2 * core + piece
+                source = wg.at[sent, place] if step else w.at[:, aligned(place, quarter)]
                 ring[side, step, piece] = remote(
-                    source, wg.at[sent, core, span],
+                    source, wg.at[sent, place],
                     ring_send.at[side, step, piece], ring_recv.at[side, step, piece], me, target)
-                span = pl.ds(start, spans[piece][1])
                 swap_weight[side, step, piece] = remote(
-                    wg.at[came, core, span], wg.at[came, core, span],
+                    wg.at[came, place], wg.at[came, place],
                     pair_send.at[side, step, piece], pair_recv.at[side, step, piece], partner, mine)
-        span = pl.ds(half_rows, tail_rows)
-        ring[side, "tail"] = remote(
-            wg.at[mine, core, span], wg.at[mine, core, span],
-            ring_send.at[side, steps, 0], ring_recv.at[side, steps, 0], me, target)
 
     events = [(step, piece) for step in range(steps - 1) for piece in range(2)]
 
@@ -155,8 +135,6 @@
             step, piece = events[n]
             for side in range(2):
                 ring[side, step, piece].wait_recv()
-                if step == 0 and piece == 1:
-                    ring[side, "tail"].wait_recv()
                 if (side, step + 1, piece) in ring:
                     ring[side, step + 1, piece].start()
                 swap_weight[side, step, piece].start()
@@ -166,38 +144,30 @@
                 swap_weight[side, steps - 1, side].start()
 
     pl.semaphore_wait(barrier, 5)
+    for side in range(2):
+        ring[side, 0, 0].start()
+
+    @pl.when(chip == 1)
+    def _():
+        for a in range(2):
+            query_sends[0, a].start()
+
     for copy in gate_copies + swap_copies:
         copy.start()
 
     @pl.when(chip == 1)
     def _():
-        for p in range(pairs):
+        for p in range(1, pairs):
             for a in range(2):
                 query_sends[p, a].start()
 
-    for piece in range(2):
-        for side in range(2):
-            ring[side, 0, piece].start()
+    for side in range(2):
+        ring[side, 0, 1].start()
     for copy in local_copies + own_copies:
         copy.start()
     gates_all[me] = gate[...]
 
-    whole_w.wait()
-    quarter = half_rows // 2
     nt = (((1,), (1,)), ((), ()))
-    picked = lax.broadcasted_iota(jnp.int32, (tail_rows, tail_columns), 0)
-    column = lax.broadcasted_iota(jnp.int32, (tail_rows, tail_columns), 1)
-    for half in range(2):
-        packed = jnp.zeros((tail_rows, quarter), jnp.float32)
-        for a in range(2):
-            chosen = jnp.where(picked == column + a * tail_columns, 1.0, 0.0).astype(jnp.bfloat16)
-            first = half * half_rows + a * quarter
-            packed += lax.dot_general(
-                chosen, wfull[first:first + quarter, main:], nt, preferred_element_type=jnp.float32)
-        wg[mine, half, half_rows:, :] = packed.astype(jnp.bfloat16)
-    for side in range(2):
-        ring[side, "tail"].start()
-
     log2e = math.log2(math.e)
     factor = depth ** -0.5 * log2e
     lane = lax.broadcasted_iota(jnp.int32, (tokens, LANES), 1)
@@ -261,14 +231,12 @@
                 parts = block(p, qg[first:first + tokens, pair_columns(p)], first + tokens, True, first, 0)
                 done_out[first:first + tokens, pair_columns(p)] = by_head(
                     [weighted / total for weighted, _, total in parts]).astype(jnp.bfloat16)
-            if p == pairs // 2 - 1:
-                ring_event(0)
         final_copy.start()
         final_local.start()
-        ring_event(1)
+        ring_event(0)
         for p in range(pairs):
             if p == pairs // 2:
-                ring_event(2)
+                ring_event(1)
             for c in range(2):
                 query_recvs[p, c].wait_recv()
             for i in range(2):
@@ -280,8 +248,8 @@
                 sx[p, i] = jnp.transpose(stats_of(parts))[:8, :]
                 cross_sends[p, i].start()
                 stat_sends[p, i].start()
+        ring_event(2)
         ring_event(3)
-        ring_event(4)
         for copy in list(cross_sends.values()) + list(stat_sends.values()):
             copy.wait_send()
 
@@ -296,16 +264,13 @@
                     chip_rows + first, chip_rows)
                 local_f32[first:first + tokens, pair_columns(p)] = by_head([part[0] for part in parts])
                 local_stats[p, first:first + tokens, :] = stats_of(parts)
-            if p == pairs // 2 - 1:
-                ring_event(0)
+        ring_event(0)
         ring_event(1)
         for p in range(pairs):
             if p == 1:
                 ring_event(2)
-            if p == 2:
+            if p == pairs - 1:
                 ring_event(3)
-            if p == 3:
-                ring_event(4)
             for i in range(2):
                 first = i * tokens
                 cross_sends[p, i].wait_recv()
@@ -331,39 +296,35 @@
         for copy in query_sends.values():
             copy.wait_send()
 
-    for n in range(5, len(events) + 1):
-        ring_event(n)
-
+    def project(owner):
+        product = jnp.zeros((columns, tokens), jnp.float32)
+        for n in range(4):
+            product += lax.dot_general(
+                wg[owner, n], attended[:, n * quarter:(n + 1) * quarter], nt,
+                preferred_element_type=jnp.float32)
+        out[pl.ds(pl.multiple_of(owner * columns, 8), columns), :] = product.astype(jnp.bfloat16)
+
+    def project_step(step):
+        for side in range(2):
+            for piece in range(2):
+                if step < steps - 1 or piece == side:
+                    swap_weight[side, step, piece].wait()
+        for side in range(2 if step < steps - 1 else 1):
+            project(came_from[side, step])
+
+    ring_event(4)
     for copy in own_copies:
         copy.wait()
     final_local.wait()
     final_copy.wait()
-    for copy in swap_weight.values():
-        copy.wait()
-
-    tail_first = jnp.zeros((tokens, dp * tail_rows), jnp.float32)
-    tail_second = jnp.zeros((tokens, dp * tail_rows), jnp.float32)
-    for half in range(2):
-        packed = wg[:, half, half_rows:, :].reshape(dp * tail_rows, main)
-        tail_first += lax.dot_general(
-            attended[:, half * half_rows:half * half_rows + quarter], packed, nt,
-            preferred_element_type=jnp.float32)
-        tail_second += lax.dot_general(
-            attended[:, half * half_rows + quarter:(half + 1) * half_rows], packed, nt,
-            preferred_element_type=jnp.float32)
-    for owner in range(dp):
-        product = jnp.dot(
-            attended[:, :half_rows], wg[owner, 0, :half_rows, :], preferred_element_type=jnp.float32)
-        product += jnp.dot(
-            attended[:, half_rows:], wg[owner, 1, :half_rows, :], preferred_element_type=jnp.float32)
-        first = owner * tail_rows
-        second = first + tail_columns
-        end = (
-            tail_first[:, first:first + tail_columns]
-            + tail_second[:, second:second + tail_columns]
-        )
-        whole = jnp.concatenate([product, end], axis=1).astype(jnp.bfloat16)
-        out[:, owner * columns:(owner + 1) * columns] = whole
+    project(mine)
+    project_step(0)
+    ring_event(5)
+    project_step(1)
+    for n in range(6, len(events) + 1):
+        ring_event(n)
+    for step in range(2, steps):
+        project_step(step)
 
     for copy in gate_copies + swap_copies + list(ring.values()):
         copy.wait_send()
@@ -372,7 +333,6 @@
 def fused(dp, depth, q, k, v, gate, w):
     tokens, width = q.shape
     columns = w.shape[1]
-    main = columns // LANES * LANES
     half = width // 2
     pairs = half // LANES
     steps = dp // 2
@@ -383,7 +343,7 @@
     stats = pltpu.VMEM((pairs, 2, 8, tokens), jnp.float32)
     return pl.pallas_call(
         functools.partial(fused_kernel, dp, depth),
-        out_shape=jax.ShapeDtypeStruct((tokens, columns * dp), jnp.bfloat16),
+        out_shape=jax.ShapeDtypeStruct((columns * dp, tokens), jnp.bfloat16),
         in_specs=[any_spec, any_spec, any_spec, vmem_spec, any_spec],
         out_specs=vmem_spec,
         scratch_shapes=[
@@ -393,30 +353,27 @@
             held, held, stats, stats, held,
             pltpu.VMEM((tokens, width), jnp.bfloat16),
             pltpu.VMEM((4,) + gate.shape, jnp.float32),
-            pltpu.VMEM(w.shape, jnp.bfloat16),
-            pltpu.VMEM((dp, 2, half + SUBLANES, main), jnp.bfloat16),
+            pltpu.VMEM((dp, 4, columns, width // 4), jnp.bfloat16),
             dma((3,)), dma((3,)), dma((3,)), dma((3,)), dma((3,)),
             dma((pairs, 2)), dma((pairs, 2)),
             dma((pairs, 2)), dma((pairs, 2)), dma((pairs, 2)), dma((pairs, 2)),
             dma((1,)), dma((1,)), dma((1,)),
-            dma((2, steps + 1, 2)), dma((2, steps + 1, 2)),
-            dma((2, steps, 2)), dma((2, steps, 2)), dma((3,)),
+            dma((2, steps, 2)), dma((2, steps, 2)),
+            dma((2, steps, 2)), dma((2, steps, 2)), dma((4,)),
         ],
         compiler_params=pltpu.CompilerParams(
-            collective_id=0, has_side_effects=True, vmem_limit_bytes=48 * 1024 * 1024),
-    )(q, k, v, gate, w)
+            collective_id=0, has_side_effects=True, vmem_limit_bytes=60 * 1024 * 1024),
+    )(q, k, v, gate, w.T).T
 
 
 def fits(sp, dp, tokens, width, depth, columns):
-    main = columns // LANES * LANES
     return (
         sp == 4 and dp % 2 == 0 and 8 <= dp <= 16
-        and width % (2 * LANES) == 0 and width <= 1024 and LANES % depth == 0
+        and width % (4 * LANES) == 0 and width <= 1024 and LANES % depth == 0
         and tokens <= 256 and tokens % LANES == 0
         and (width // depth // sp) % (LANES // depth) == 0
         and LANES // depth <= 4
-        and main * 4 == width and columns > main
-        and 2 * (columns - main) == SUBLANES
+        and columns % 8 == 0 and columns * dp <= 4096
     )
 
 

time: 41.2 us -> 46 us (1.12)
  the two profiles are of different devices: /device:TPU:0 before, /device:TPU:13 now
where the time goes in v3:
time: 46 us; the launch traced here: 45.8 us
  Pallas kernels  43.5 us (95%)
  local copies, waits for them, and re-layouts  2.29 us (5%)
    pallas_call x1, Pallas kernels, fused(): pl.pallas_call(functools.partial(fused_kernel, dp, depth), out_shape=jax....  43.5 us
    unnamed x1, local copies, waits for them, and re-layouts  2.29 us

profile of v3, /device:TPU:13, one launch (start us, length us, event | category | flops | bytes accessed | tf_op | source)
XLA Modules:
  0.0 45.8 jit_solution(14223457739122346608)
XLA Ops:
  0.0 43.5 %shard_map.55 = bf16[2112,256]{1,0:T(8,128)(2,1)} custom-call(bf16[256,1024]{1,0:T(8,128)(2,1)} %bitcast.10, bf16[256,1024]{1,0:T(8,128)(2,1)} %bitcast.11, bf16[256,1024]{1,0:T(8,128)(2,1)} %bitcast.12, f32[4,1024]{1,0:T(4,128)} %bitcast.13, bf16[264,1024]{1,0:T(8,128)(2,1)} %bitcast.9), custom_call_target="tpu_custom_call" | custom-call | tf_op jit(solution)/shard_map/pallas_call | solution.py:344
  43.5 2.3 %copy.7 = bf16[1,256,2112]{1,2,0:T(8,128)(2,1)} copy(bf16[1,256,2112]{1,2,0:T(8,128)(2,1)} %bitcast.8) | data formatting | bytes 2162688
